TPU v7x, 256 devices: a whole 4x4x8 slice. The times are simulated.
256 devices in a mesh: dp: 4 (over x), kv: 32 (over z, y), tp: 2 (over core).
Axes of the slice: x: 4, y: 4, z: 8, core: 2. Of those that a mesh axis runs over, the one named last changes fastest.
Arguments:
- tokens: bfloat16 [4, 8192, 2048], P('dp', 'kv'), may hold values from -28 to 28, as said below
- query_weight: bfloat16 [2048, 768], P(None, 'tp'), may hold values from -0.125 to 0.125
- key_weight: bfloat16 [2048, 256], P(None, 'tp'), may hold values from -0.125 to 0.125
- value_weight: bfloat16 [2048, 256], P(None, 'tp'), may hold values from -0.125 to 0.125
- gate_weight: bfloat16 [2048, 24], replicated, may hold values from -0.125 to 0.125
- compress_weight: float32 [2, 32, 64], replicated, may hold values from -1 to 1
- out_weight: bfloat16 [768, 2048], P('tp'), may hold values from -0.21875 to 0.21875
- out_gain: float32 [2048], replicated, may hold values from 0.1 to 1.9
- chosen: int32 [4, 256, 16], P('dp', 'kv'), may hold values from -1 to 255, as said below
Outputs:
- output: float32 [4, 8192, 2048], P('dp', ('kv', 'tp'))
Inputs may be any that keep to these rules, and one draw needn't show every extreme that they name: `chosen`: row q of a sequence lists distinct blocks; its first entry is q itself; the others are -1 or blocks held by an earlier index of kv (block index // 8). Over the rows of one kv index, at most 2 distinct blocks come from any other single index, and every index past the first reads exactly 2 blocks of the first index, among them block 0. `tokens`: finite activations; some rows are much larger than others in some draws.
All inputs are finite; a program needn't handle non-finite values.
Results may differ from a plain program's by a relative error of at most 0.02.
The roundings to bfloat16 on the way count: a program that leaves them out, or rounds other values in their place, can miss the bound.
Values may be sent and summed in bfloat16 or wider, within the bound.
No kernel may reach another device: no remote copies, remote signals or barrier semaphores. Data moves between devices by JAX's collectives and lax.ppermute only.
A program may use at most 64 MiB of HBM per device.

v0:
```python
import jax
import jax.numpy as jnp
from jax import lax
from jax.experimental import pallas as pl
from jax.experimental.pallas import tpu as pltpu
from jax.sharding import PartitionSpec as P


HEAD = 64
BLK = 32
TOPN = 16
NEG = -1e30
ROPE_BASE = 500000.0
EPS = 1e-06
Z, Y = 8, 4
UNIT = 528
SHARE = 576
PIECE = 144
BF = jnp.bfloat16
F32 = jnp.float32


def dot(a, b):
    return jnp.dot(a, b, preferred_element_type=F32)


def dot_t(a, b):
    return lax.dot_general(a, b, (((1,), (1,)), ((), ())), preferred_element_type=F32)


def turn(x, cosine, sine):
    lane = lax.broadcasted_iota(jnp.int32, x.shape, 1)
    other = jnp.where(lane % HEAD < HEAD // 2, pltpu.roll(x, 96, 1), pltpu.roll(x, 32, 1))
    return x * cosine + other * sine


def kv_kernel(after_ref, x_ref, wk_ref, wv_ref, cw_ref, cos_ref, sin_ref, out_ref):
    x = x_ref[...]
    keys = dot(x, wk_ref[...]).astype(BF).astype(F32)
    out_ref[pl.ds(0, 256), :] = turn(keys, cos_ref[...], sin_ref[...]).astype(BF)
    values = dot(x, wv_ref[...]).astype(BF)
    out_ref[pl.ds(256, 256), :] = values

    def compress(rows, weight):
        wide = jnp.concatenate([weight, weight], axis=1)
        return jnp.sum(rows.reshape(8, BLK, 128) * wide[None], axis=1)

    packed = jnp.concatenate(
        [compress(keys, cw_ref[0]), compress(values.astype(F32), cw_ref[1])], axis=0
    )
    out_ref[pl.ds(512, 16), :] = packed.astype(BF)


def table_kernel(scalar_ref, listed_ref, ask_ref, rows_ref, bias_ref):
    z = lax.axis_index("kv") // Y
    listed = listed_ref[...]
    lane = lax.broadcasted_iota(jnp.int32, (8, 128), 1)
    low, high = jnp.full((8, 128), 7, jnp.int32), jnp.zeros((8, 128), jnp.int32)
    for g in range(4):
        row = jnp.zeros((8, 128), F32)
        for part in range(4):
            entry = jnp.broadcast_to(listed[:, g * 4 + part : g * 4 + part + 1], (8, 128))
            hit = (entry >> 3) == lane
            low = jnp.minimum(low, jnp.where(hit, entry & 7, 7))
            high = jnp.maximum(high, jnp.where(hit, entry & 7, 0))
            row = jnp.where((lane >> 5) == part, jnp.where(entry >= 0, 0.0, NEG), row)
        bias_ref[:, pl.ds(g * 128, 128)] = row
    low = jnp.min(low, axis=0, keepdims=True)
    high = jnp.max(high, axis=0, keepdims=True)
    first = lax.broadcasted_iota(jnp.int32, (8, 128), 0) == 0
    ask_ref[...] = jnp.where(first, low, high)
    owner = listed >> 3
    second = jnp.zeros((8, TOPN), jnp.int32)
    for i in range(8):
        for t in range(TOPN):
            other = scalar_ref[i, t]
            second = jnp.where((owner == (other >> 3)) & (other < listed), 1, second)
    owner = jnp.maximum(listed, 0) >> 3
    owner_z = owner >> 2
    sender = (z // 2) * 2 + (owner_z & 1)
    u = ((sender - owner_z) & 7) >> 1
    rows_ref[...] = ((owner_z & 1) * Y + (owner & 3)) * SHARE + u * PIECE + second * BLK


def q_kernel(
    x_ref, wq_ref, wg_hbm, cos_ref, sin_ref, plain_ref, turned_ref, gate_ref, wg_ref, sem
):
    copy = pltpu.make_async_copy(wg_hbm, wg_ref, sem)
    copy.start()
    x = x_ref[...]
    lane = lax.broadcasted_iota(jnp.int32, (256, 128), 1)
    for pair in range(3):
        q = dot(x, wq_ref[:, pl.ds(pair * 128, 128)]).astype(BF).astype(F32)
        t = turn(q, cos_ref[...], sin_ref[...]).astype(BF).astype(F32)
        for half in range(2):
            head = pair * 2 + half
            side = head // 3
            keep = (lane >= HEAD) if side else (lane < HEAD)
            for src, dst in ((q, plain_ref), (t, turned_ref)):
                rows = src if half == side else pltpu.roll(src, 64, 1)
                rows = jnp.where(keep, rows * 0.125, 0.0).astype(BF)
                for i in range(8):
                    dst[i, pl.ds(head * BLK, BLK), :] = rows[i * BLK : (i + 1) * BLK]
    copy.wait()
    gate_ref[...] = jax.nn.sigmoid(dot(x, wg_ref[...]))


def select_kernel(*refs):
    asks, units, out = refs[:Y], refs[Y : Y + 4], refs[Y + 4]
    index = lax.axis_index("kv")
    z, y = index // Y, index % Y
    for d in range(Y):
        for partner in range(2):
            dest = lax.rem(z + partner, 2) * Y + lax.rem(y + d, Y)
            for u in range(4):
                base = pl.multiple_of(dest * SHARE + u * PIECE, 16)
                source = lax.rem(z - 2 * u + Z, Z) * Y + y
                for slot in range(2):
                    row = pl.multiple_of(asks[d][partner * 8 + slot, source] * BLK, BLK)
                    out[pl.ds(base + slot * BLK, BLK), :] = units[u][pl.ds(row, BLK), :]
                    out[pl.ds(base + 64 + slot * BLK, BLK), :] = units[u][pl.ds(row + 256, BLK), :]
                out[pl.ds(base + 128, 16), :] = units[u][pl.ds(512, 16), :]


def attend_kernel(
    row_ref, bias_ref, plain_ref, turned_ref, gate_ref, unit_ref, pool, *refs
):
    keep_ref, send_ref, sk, sv, kg, vg = refs
    index = lax.axis_index("kv")
    z, y, core = index // Y, index % Y, lax.axis_index("tp")
    for piece in range(32):
        base = piece * PIECE + 128
        sk[pl.ds(piece * 8, 8), :] = pool[pl.ds(base, 8), :]
        sv[pl.ds(piece * 8, 8), :] = pool[pl.ds(base + 8, 8), :]

    column = lax.broadcasted_iota(jnp.int32, (192, 256), 1)
    row = lax.broadcasted_iota(jnp.int32, (192, 256), 0) % BLK
    sender = (z // 2) * 2 + column // 128
    dev = ((sender - 2 * (column // 8 % 4) + Z) % Z) * Y + column // 32 % Y
    block_id = dev * 8 + column % 8
    own_first = (z * Y + y) * 8
    triangle = jnp.where(
        (column[:, :128] < BLK) & (column[:, :128] > row[:, :128]), NEG, 0.0
    )
    lane = lax.broadcasted_iota(jnp.int32, (BLK, 128), 1)
    coarse_keys, coarse_values = sk[...], sv[...]

    for step in range(8):
        i = lax.rem(step + 4 * (1 - core), 8)
        own_row = pl.multiple_of(i * BLK, BLK)
        kg[step % 2, pl.ds(0, BLK), :] = unit_ref[pl.ds(own_row, BLK), :]
        vg[step % 2, pl.ds(0, BLK), :] = unit_ref[pl.ds(own_row + 256, BLK), :]
        for t in range(1, TOPN):
            at = pl.multiple_of(row_ref[i, t], 16)
            kg[step % 2, pl.ds(t * BLK, BLK), :] = pool[pl.ds(at, BLK), :]
            vg[step % 2, pl.ds(t * BLK, BLK), :] = pool[pl.ds(at + 64, BLK), :]
        scores = dot_t(plain_ref[i], coarse_keys)
        own = own_first + i
        visible = (block_id < own) | ((block_id == own) & (row == BLK - 1))
        scores = jnp.where(visible, scores, NEG)
        peak = jnp.max(scores, axis=-1, keepdims=True)
        powers = jnp.where(visible, jnp.exp(scores - peak), 0.0)
        total = jnp.maximum(jnp.sum(powers, axis=-1, keepdims=True), 1.0)
        weight = (powers * (1.0 / total)).astype(BF)
        coarse = dot(weight, coarse_values)

        fine = dot_t(turned_ref[i], kg[step % 2]) + bias_ref[pl.ds(i, 1), :]
        fine = jnp.concatenate([fine[:, :128] + triangle, fine[:, 128:]], axis=1)
        fine_peak = jnp.max(fine, axis=-1, keepdims=True)
        fine_powers = jnp.exp(fine - fine_peak)
        fine_total = jnp.sum(fine_powers, axis=-1, keepdims=True)
        fine_out = dot(fine_powers.astype(BF), vg[step % 2]) * (1.0 / fine_total)

        gates = gate_ref[pl.ds(pl.multiple_of(i * BLK, BLK), BLK), :]
        heads = []
        for head in range(6):
            pick = []
            for base in (0, 12):
                low = gates[:, base + head : base + head + 1]
                high = gates[:, base + 6 + head : base + 7 + head]
                pick.append(jnp.where(core == 0, low, high))
            span = slice(head * BLK, (head + 1) * BLK)
            heads.append(pick[0] * coarse[span] + pick[1] * fine_out[span])
        groups = (
            jnp.where(lane < HEAD, heads[0], pltpu.roll(heads[1], 64, 1)),
            jnp.where(lane < HEAD, heads[2], heads[3]),
            jnp.where(lane < HEAD, pltpu.roll(heads[4], 64, 1), heads[5]),
        )
        target = send_ref if step < 4 else keep_ref
        for g in range(3):
            target[pl.ds((step % 4) * BLK, BLK), pl.ds(g * 128, 128)] = groups[g].astype(BF)


def out_kernel(keep_ref, got_ref, w_own_ref, w_other_ref, gain_ref, out_ref):
    summed = dot(keep_ref[...], w_own_ref[...]) + dot(got_ref[...], w_other_ref[...])
    mean = jnp.mean(summed * summed, axis=-1, keepdims=True)
    out_ref[...] = summed * lax.rsqrt(mean + EPS) * gain_ref[...]


VMEM = pl.BlockSpec(memory_space=pltpu.VMEM)
HBM = pl.BlockSpec(memory_space=pltpu.HBM)
SMEM = pl.BlockSpec(memory_space=pltpu.SMEM)


def call(kernel, out_shape, specs, args, scratch=(), flops=0, data=0, vmem=12 * 2**20):
    return pl.pallas_call(
        kernel,
        out_shape=out_shape,
        in_specs=specs,
        out_specs=jax.tree.map(lambda _: VMEM, out_shape),
        scratch_shapes=scratch,
        compiler_params=pltpu.CompilerParams(vmem_limit_bytes=vmem),
        cost_estimate=pl.CostEstimate(flops=flops, bytes_accessed=data, transcendentals=0),
    )(*args)


def z_shift(d):
    return [(z * Y + y, (z + d) % Z * Y + y) for z in range(Z) for y in range(Y)]


def y_shift(d):
    return [(z * Y + y, z * Y + (y + d) % Y) for z in range(Z) for y in range(Y)]


def z_pair():
    return [(z * Y + y, (z ^ 1) * Y + y) for z in range(Z) for y in range(Y)]


def pair_groups():
    return [[(2 * p + a) * Y + y for a in range(2) for y in range(Y)] for p in range(Z // 2)]


def rope_tables(positions):
    half = HEAD // 2
    inverse = ROPE_BASE ** (-jnp.arange(half, dtype=F32) * (2.0 / HEAD))
    angles = positions.astype(F32)[:, None] * inverse[None, :]
    cosine, sine = jnp.cos(angles), jnp.sin(angles)
    return (
        jnp.concatenate([cosine] * 4, axis=-1),
        jnp.concatenate([-sine, sine, -sine, sine], axis=-1),
    )


def on_device(
    tokens,
    query_weight,
    key_weight,
    value_weight,
    gate_weight,
    compress_weight,
    out_weight,
    out_gain,
    chosen,
):
    shape = jax.ShapeDtypeStruct
    x = tokens[0]
    index = lax.axis_index("kv")
    other_weight = lax.ppermute(out_weight, "tp", [(0, 1), (1, 0)])
    ask, rows, bias = call(
        table_kernel,
        (
            shape((8, 128), jnp.int32),
            shape((8, TOPN), jnp.int32),
            shape((8, TOPN * BLK), F32),
        ),
        [SMEM, VMEM],
        (chosen[0], chosen[0]),
        flops=2**32,
        data=2**12,
    )
    partner_ask = lax.ppermute(ask, "kv", z_pair())

    cosine, sine = rope_tables(index * 256 + jnp.arange(256, dtype=jnp.int32))
    unit = call(
        kv_kernel,
        shape((UNIT, 128), BF),
        [VMEM] * 7,
        (ask, x, key_weight, value_weight, compress_weight, cosine, sine),
        flops=2 * 256 * 2048 * 256,
        data=2 * 2**20,
    )
    units = [unit] + [lax.ppermute(unit, "kv", z_shift(d)) for d in (2, 4, 6)]
    asks = jnp.concatenate([ask, partner_ask])
    asks = [asks] + [lax.ppermute(asks, "kv", y_shift(-d)) for d in (1, 2, 3)]

    plain, turned, gates = call(
        q_kernel,
        (shape((8, 192, 128), BF), shape((8, 192, 128), BF), shape((256, 24), F32)),
        [VMEM, VMEM, HBM, VMEM, VMEM],
        (x, query_weight, gate_weight, cosine, sine),
        scratch=[pltpu.VMEM(gate_weight.shape, BF), pltpu.SemaphoreType.DMA],
        flops=2 * 256 * 2048 * 408,
        data=3 * 2**20,
    )
    share = call(
        select_kernel,
        shape((8 * SHARE, 128), BF),
        [SMEM] * 4 + [VMEM] * 4,
        (*asks, *units),
        flops=2**20,
        data=2 * 2**20,
    )
    pool = lax.all_to_all(
        share.reshape(8, SHARE, 128), "kv", 0, 0, tiled=True, axis_index_groups=pair_groups()
    ).reshape(8 * SHARE, 128)

    keep, send = call(
        attend_kernel,
        (shape((128, 384), BF), shape((128, 384), BF)),
        [SMEM] + [VMEM] * 6,
        (rows, bias, plain, turned, gates, unit, pool),
        scratch=[
            pltpu.VMEM((256, 128), BF),
            pltpu.VMEM((256, 128), BF),
            pltpu.VMEM((2, 512, 128), BF),
            pltpu.VMEM((2, 512, 128), BF),
        ],
        flops=2**30,
        data=4 * 2**20,
        vmem=58720256,
    )
    got = lax.ppermute(send, "tp", [(0, 1), (1, 0)])
    out = call(
        out_kernel,
        shape((128, 2048), F32),
        [VMEM] * 5,
        (keep, got, out_weight, other_weight, out_gain[None]),
        flops=2 * 128 * 768 * 2048,
        data=4 * 2**20,
    )
    return out[None]


def solution(mesh):
    in_specs = (
        P("dp", "kv", None),
        P(None, "tp"),
        P(None, "tp"),
        P(None, "tp"),
        P(),
        P(),
        P("tp", None),
        P(),
        P("dp", "kv", None),
    )
    out_specs = P("dp", ("kv", "tp"), None)

    return jax.shard_map(
        on_device, mesh=mesh, in_specs=in_specs, out_specs=out_specs, check_vma=False
    )
```

profile of v0, /device:TPU:1, one launch (start us, length us, event | category | flops | bytes accessed | tf_op | source)
XLA Modules:
  0.0 69.3 jit_solution(15954209105744317554)
XLA Ops:
  0.0 0.0 copy-start.12
  0.0 0.7 copy-done.12
  0.7 0.8 %shard_map.91 = (s32[8,128]{1,0:T(8,128)S(1)}, s32[8,16]{1,0:T(8,128)S(1)}, f32[8,512]{1,0:T(8,128)S(1)}) custom-call(s32[8,16]{1,0:T(8,128)S(1)} %bitcast.9, s32[8,16]{1,0:T(8,128)S(1)} %bitcast.10), custom_call_target="tpu_custom_call" | custom-call | flops 4294967296 | bytes 4096 | tf_op jit(solution)/shard_map/pallas_call | solution.py:206
  1.5 0.0 copy-start.13
  1.5 0.0 copy-start.14
  1.5 0.0 copy-start
  1.5 0.5 fusion
  2.1 0.0 copy-done.13
  2.1 0.0 copy-done.14
  2.1 0.3 pad_maximum_fusion
  2.4 0.0 copy-done.4
  2.4 0.4 copy-done
  2.8 0.7 %shard_map.93.refs_4_.unit_ref = bf16[528,128]{1,0:T(8,128)(2,1)S(1)} custom-call(s32[8,128]{1,0:T(8,128)S(1)} %get-tuple-element.18.after_ref, bf16[256,2048]{1,0:T(8,128)(2,1)S(1)} %bitcast.6, bf16[2048,128]{1,0:T(8,128)(2,1)S(1)} %copy-done.4, bf16[2048,128]{1,0:T(8,128)(2,1)S(1)} %copy-done.5, f32[2,32,64]{2,1,0:T(8,128)S(1)} %copy-done.7, ...), custom_call_target="tpu_custom_call" | custom-call | flops 268435456 | bytes 2097152 | tf_op jit(solution)/shard_map/pallas_call | solution.py:206
  3.5 0.0 copy-start.3
  3.6 3.9 %collective-permute-start.4 = (bf16[528,128]{1,0:T(8,128)(2,1)S(1)}, bf16[528,128]{1,0:T(8,128)(2,1)S(1)}, u32[]{:S(2)}, u32[]{:S(2)}) collective-permute-start(bf16[528,128]{1,0:T(8,128)(2,1)S(1)} %shard_map.93.refs_4_.unit_ref), channel_id=1, source_target_pairs={{0,16},{2,18},{4,20},{6,22},{8,24},{10,26},{12,28},{14,30},{16,32}... | collective-permute-start | bytes 405512 | tf_op jit(solution)/shard_map/ppermute | solution.py:282
  7.4 5.1 %collective-permute-start.5 = (bf16[528,128]{1,0:T(8,128)(2,1)S(1)}, bf16[528,128]{1,0:T(8,128)(2,1)S(1)}, u32[]{:S(2)}, u32[]{:S(2)}) collective-permute-start(bf16[528,128]{1,0:T(8,128)(2,1)S(1)} %shard_map.93.refs_4_.unit_ref), channel_id=1, source_target_pairs={{0,32},{2,34},{4,36},{6,38},{8,40},{10,42},{12,44},{14,46},{16,48}... | collective-permute-start | bytes 405512 | tf_op jit(solution)/shard_map/ppermute | solution.py:282
  12.6 2.4 %collective-permute-start.6 = (bf16[528,128]{1,0:T(8,128)(2,1)S(1)}, bf16[528,128]{1,0:T(8,128)(2,1)S(1)}, u32[]{:S(2)}, u32[]{:S(2)}) collective-permute-start(bf16[528,128]{1,0:T(8,128)(2,1)S(1)} %shard_map.93.refs_4_.unit_ref), channel_id=1, source_target_pairs={{0,48},{2,50},{4,52},{6,54},{8,56},{10,58},{12,60},{14,62},{16,0},... | collective-permute-start | bytes 405512 | tf_op jit(solution)/shard_map/ppermute | solution.py:282
  14.9 0.7 %collective-permute-start = (s32[8,128]{1,0:T(8,128)S(1)}, s32[8,128]{1,0:T(8,128)S(1)}, u32[]{:S(2)}, u32[]{:S(2)}) collective-permute-start(s32[8,128]{1,0:T(8,128)S(1)} %get-tuple-element.18.after_ref), channel_id=1, source_target_pairs={{0,8},{2,10},{4,12},{6,14},{8,0},{10,2},{12,4},{14,6},{16,24},{18,... | collective-permute-start | bytes 12296 | tf_op jit(solution)/shard_map/ppermute | solution.py:271
  15.7 8.1 %collective-permute-done = s32[8,128]{1,0:T(8,128)S(1)} collective-permute-done((s32[8,128]{1,0:T(8,128)S(1)}, s32[8,128]{1,0:T(8,128)S(1)}, u32[]{:S(2)}, u32[]{:S(2)}) %collective-permute-start) | collective-permute-done | bytes 4128 | tf_op jit(solution)/shard_map/ppermute | solution.py:271
  23.8 2.7 %collective-permute-start.1 = (s32[16,128]{1,0:T(8,128)S(1)}, s32[16,128]{1,0:T(8,128)S(1)}, u32[]{:S(2)}, u32[]{:S(2)}) collective-permute-start(s32[16,128]{1,0:T(8,128)S(1)} %constant_dynamic-update-slice_fusion.refs_0_), channel_id=1, source_target_pairs={{0,6},{2,0},{4,2},{6,4},{8,14},{10,8},{12,10},{14,12},{16,22},{18,... | collective-permute-start | bytes 24584 | tf_op jit(solution)/shard_map/ppermute | solution.py:284
  26.5 0.3 collective-permute-start.2
  26.9 0.4 collective-permute-done.1.refs_1_
  27.3 0.3 collective-permute-start.3
  27.6 2.9 %collective-permute-done.2.refs_2_ = s32[16,128]{1,0:T(8,128)S(1)} collective-permute-done((s32[16,128]{1,0:T(8,128)S(1)}, s32[16,128]{1,0:T(8,128)S(1)}, u32[]{:S(2)}, u32[]{:S(2)}) %collective-permute-start.2) | collective-permute-done | bytes 8224 | tf_op jit(solution)/shard_map/ppermute | solution.py:284
  30.5 0.7 %collective-permute-done.3.refs_3_ = s32[16,128]{1,0:T(8,128)S(1)} collective-permute-done((s32[16,128]{1,0:T(8,128)S(1)}, s32[16,128]{1,0:T(8,128)S(1)}, u32[]{:S(2)}, u32[]{:S(2)}) %collective-permute-start.3) | collective-permute-done | bytes 8224 | tf_op jit(solution)/shard_map/ppermute | solution.py:284
  31.3 0.0 collective-permute-done.4.refs_5_
  31.3 0.0 collective-permute-done.5.refs_6_
  31.3 0.0 collective-permute-done.6.refs_7_
  31.3 2.6 %shard_map.94 = bf16[4608,128]{1,0:T(8,128)(2,1)} custom-call(s32[16,128]{1,0:T(8,128)S(1)} %constant_dynamic-update-slice_fusion.refs_0_, s32[16,128]{1,0:T(8,128)S(1)} %collective-permute-done.1.refs_1_, s32[16,128]{1,0:T(8,128)S(1)} %collective-permute-done.2.refs_2_, s32[16,128]{1,0:T(8,128)S(1)} %collective-permute-done.3.refs_3_, ...), custom_call_target="tpu_custom_call" | custom-call | flops 1048576 | bytes 2097152 | tf_op jit(solution)/shard_map/pallas_call | solution.py:206
  34.0 4.4 %all-to-all-start = ((bf16[8,576,128]{2,1,0:T(8,128)(2,1)}), bf16[8,576,128]{2,1,0:T(8,128)(2,1)}, u32[]{:S(2)}, u32[]{:S(2)}) async-start(bf16[8,576,128]{2,1,0:T(8,128)(2,1)} %bitcast.2), calls=%async_computation | async-start | bytes 2359296 | tf_op jit(solution)/shard_map/all_to_all | solution.py:303
  38.4 0.0 copy-done.1
  38.4 3.1 %collective-permute-start.8 = (bf16[384,2048]{1,0:T(8,128)(2,1)S(1)}, bf16[384,2048]{1,0:T(8,128)(2,1)}, u32[]{:S(2)}, u32[]{:S(2)}) collective-permute-start(bf16[384,2048]{1,0:T(8,128)(2,1)S(1)} %copy-done.1), channel_id=1, source_target_pairs={{0,1},{1,0},{2,3},{3,2},{4,5},{5,4},{6,7},{7,6},{8,9},{9,8},{10,11... | collective-permute-start | bytes 4718600 | tf_op jit(solution)/shard_map/ppermute | solution.py:258
  41.5 0.0 copy-done.15
  41.5 0.3 copy.12.wg_hbm
  41.8 0.0 copy-start.2
  41.8 1.4 %copy-done.2 = bf16[2048,384]{1,0:T(8,128)(2,1)S(1)} copy-done((bf16[2048,384]{1,0:T(8,128)(2,1)S(1)}, bf16[2048,384]{1,0:T(8,128)(2,1)}, u32[]{:S(2)}) %copy-start.2) | copy-done | bytes 1572888
  43.2 1.6 %shard_map.92 = (bf16[8,192,128]{2,1,0:T(8,128)(2,1)S(1)}, bf16[8,192,128]{2,1,0:T(8,128)(2,1)S(1)}, f32[256,24]{1,0:T(8,128)S(1)}) custom-call(bf16[256,2048]{1,0:T(8,128)(2,1)S(1)} %bitcast.7, bf16[2048,384]{1,0:T(8,128)(2,1)S(1)} %copy-done.2, bf16[2048,24]{1,0:T(8,128)(2,1)S(1)} %copy.12.wg_hbm, f32[256,128]{1,0:T(8,128)S(1)} %get-tuple-element.24.cos_ref, ...), custom_call_target="tpu_custom_call" | custom-call | flops 427819008 | bytes 3145728 | tf_op jit(solution)/shard_map/pallas_call | solution.py:206
  44.8 0.0 copy-start.9
  44.8 0.7 %copy-done.9 = bf16[8,192,128]{2,1,0:T(8,128)(2,1)} copy-done((bf16[8,192,128]{2,1,0:T(8,128)(2,1)}, bf16[8,192,128]{2,1,0:T(8,128)(2,1)S(1)}, u32[]{:S(2)}) %copy-start.9) | copy-done | bytes 393240
  45.6 0.8 %copy-done.10 = bf16[8,192,128]{2,1,0:T(8,128)(2,1)} copy-done((bf16[8,192,128]{2,1,0:T(8,128)(2,1)}, bf16[8,192,128]{2,1,0:T(8,128)(2,1)S(1)}, u32[]{:S(2)}) %copy-start.10) | copy-done | bytes 393240
  46.3 0.6 copy-done.11
  47.0 3.8 %all-to-all-done = bf16[8,576,128]{2,1,0:T(8,128)(2,1)} async-done(((bf16[8,576,128]{2,1,0:T(8,128)(2,1)}), bf16[8,576,128]{2,1,0:T(8,128)(2,1)}, u32[]{:S(2)}, u32[]{:S(2)}) %all-to-all-start) | async-done | bytes 1179680 | tf_op jit(solution)/shard_map/all_to_all | solution.py:303
  50.8 8.5 %shard_map.95 = (bf16[128,384]{1,0:T(8,128)(2,1)}, bf16[128,384]{1,0:T(8,128)(2,1)}) custom-call(s32[8,16]{1,0:T(8,128)} %copy-done.14, f32[8,512]{1,0:T(8,128)} %copy-done.13, bf16[8,192,128]{2,1,0:T(8,128)(2,1)} %copy-done.9, bf16[8,192,128]{2,1,0:T(8,128)(2,1)} %copy-done.10, f32[256,24]{1,0:T(8,128)} %copy-done.11, bf16[528,128]{1,0:T(8,128)(2,1)} %copy-done.3, ...), custom_call_target="tpu_custom_call" | custom-call | flops 1073741824 | bytes 4194304 | tf_op jit(solution)/shard_map/pallas_call | solution.py:206
  59.2 4.7 %collective-permute-start.7 = (bf16[128,384]{1,0:T(8,128)(2,1)}, bf16[128,384]{1,0:T(8,128)(2,1)S(1)}, u32[]{:S(2)}, u32[]{:S(2)}) collective-permute-start(bf16[128,384]{1,0:T(8,128)(2,1)} %get-tuple-element.20), channel_id=1, source_target_pairs={{0,1},{1,0},{2,3},{3,2},{4,5},{5,4},{6,7},{7,6},{8,9},{9,8},{10,11... | collective-permute-start | bytes 294920 | tf_op jit(solution)/shard_map/ppermute | solution.py:322
  64.0 0.0 collective-permute-done.8.w_other_ref
  64.0 1.2 %collective-permute-done.7.got_ref = bf16[128,384]{1,0:T(8,128)(2,1)S(1)} collective-permute-done((bf16[128,384]{1,0:T(8,128)(2,1)}, bf16[128,384]{1,0:T(8,128)(2,1)S(1)}, u32[]{:S(2)}, u32[]{:S(2)}) %collective-permute-start.7) | collective-permute-done | bytes 98336 | tf_op jit(solution)/shard_map/ppermute | solution.py:322
  65.1 0.9 %copy-done.6 = bf16[128,384]{1,0:T(8,128)(2,1)S(1)} copy-done((bf16[128,384]{1,0:T(8,128)(2,1)S(1)}, bf16[128,384]{1,0:T(8,128)(2,1)}, u32[]{:S(2)}) %copy-start.6) | copy-done | bytes 98328
  66.0 3.2 %shard_map.96 = f32[128,2048]{1,0:T(8,128)} custom-call(bf16[128,384]{1,0:T(8,128)(2,1)S(1)} %copy-done.6, bf16[128,384]{1,0:T(8,128)(2,1)S(1)} %collective-permute-done.7.got_ref, bf16[384,2048]{1,0:T(8,128)(2,1)S(1)} %copy-done.1, bf16[384,2048]{1,0:T(8,128)(2,1)} %collective-permute-done.8.w_other_ref, f32[1,2048]{1,0:T(1,128)S(1)} %bitcast.8), custom_call_target="tpu_custom_call" | custom-call | flops 402653184 | bytes 4194304 | tf_op jit(solution)/shard_map/pallas_call | solution.py:206
  (17 shorter events, 0.0 us)
Async XLA Ops:
  0.0 0.7 copy-start.12
  0.7 1.6 %copy-start.4 = (bf16[2048,128]{1,0:T(8,128)(2,1)S(1)}, bf16[2048,128]{1,0:T(8,128)(2,1)}, u32[]{:S(2)}) copy-start(bf16[2048,128]{1,0:T(8,128)(2,1)} %wk_ref.1) | copy-start | bytes 1572868
  0.7 1.7 %copy-start.5 = (bf16[2048,128]{1,0:T(8,128)(2,1)S(1)}, bf16[2048,128]{1,0:T(8,128)(2,1)}, u32[]{:S(2)}) copy-start(bf16[2048,128]{1,0:T(8,128)(2,1)} %wv_ref.1) | copy-start | bytes 1572868
  0.7 1.7 %copy-start.7 = (f32[2,32,64]{2,1,0:T(8,128)S(1)}, f32[2,32,64]{2,1,0:T(8,128)}, u32[]{:S(2)}) copy-start(f32[2,32,64]{2,1,0:T(8,128)} %cw_ref.1) | copy-start | bytes 49156
  1.5 0.6 copy-start.13
  1.5 0.6 copy-start.14
  1.5 1.3 %copy-start = (bf16[1,256,2048]{2,1,0:T(8,128)(2,1)S(1)}, bf16[1,256,2048]{2,1,0:T(8,128)(2,1)}, u32[]{:S(2)}) copy-start(bf16[1,256,2048]{2,1,0:T(8,128)(2,1)} %param.9) | copy-start | bytes 3145732
  3.5 30.4 %copy-start.3 = (bf16[528,128]{1,0:T(8,128)(2,1)}, bf16[528,128]{1,0:T(8,128)(2,1)S(1)}, u32[]{:S(2)}) copy-start(bf16[528,128]{1,0:T(8,128)(2,1)S(1)} %shard_map.93.refs_4_.unit_ref) | copy-start | bytes 405508
  3.6 27.7 %collective-permute-start.4 = (bf16[528,128]{1,0:T(8,128)(2,1)S(1)}, bf16[528,128]{1,0:T(8,128)(2,1)S(1)}, u32[]{:S(2)}, u32[]{:S(2)}) collective-permute-start(bf16[528,128]{1,0:T(8,128)(2,1)S(1)} %shard_map.93.refs_4_.unit_ref), channel_id=1, source_target_pairs={{0,16},{2,18},{4,20},{6,22},{8,24},{10,26},{12,28},{14,30},{16,32}... | collective-permute-start | bytes 405512 | tf_op jit(solution)/shard_map/ppermute | solution.py:282
  7.4 23.9 %collective-permute-start.5 = (bf16[528,128]{1,0:T(8,128)(2,1)S(1)}, bf16[528,128]{1,0:T(8,128)(2,1)S(1)}, u32[]{:S(2)}, u32[]{:S(2)}) collective-permute-start(bf16[528,128]{1,0:T(8,128)(2,1)S(1)} %shard_map.93.refs_4_.unit_ref), channel_id=1, source_target_pairs={{0,32},{2,34},{4,36},{6,38},{8,40},{10,42},{12,44},{14,46},{16,48}... | collective-permute-start | bytes 405512 | tf_op jit(solution)/shard_map/ppermute | solution.py:282
  12.6 18.7 %collective-permute-start.6 = (bf16[528,128]{1,0:T(8,128)(2,1)S(1)}, bf16[528,128]{1,0:T(8,128)(2,1)S(1)}, u32[]{:S(2)}, u32[]{:S(2)}) collective-permute-start(bf16[528,128]{1,0:T(8,128)(2,1)S(1)} %shard_map.93.refs_4_.unit_ref), channel_id=1, source_target_pairs={{0,48},{2,50},{4,52},{6,54},{8,56},{10,58},{12,60},{14,62},{16,0},... | collective-permute-start | bytes 405512 | tf_op jit(solution)/shard_map/ppermute | solution.py:282
  14.9 8.9 %collective-permute-start = (s32[8,128]{1,0:T(8,128)S(1)}, s32[8,128]{1,0:T(8,128)S(1)}, u32[]{:S(2)}, u32[]{:S(2)}) collective-permute-start(s32[8,128]{1,0:T(8,128)S(1)} %get-tuple-element.18.after_ref), channel_id=1, source_target_pairs={{0,8},{2,10},{4,12},{6,14},{8,0},{10,2},{12,4},{14,6},{16,24},{18,... | collective-permute-start | bytes 12296 | tf_op jit(solution)/shard_map/ppermute | solution.py:271
  23.8 3.5 %collective-permute-start.1 = (s32[16,128]{1,0:T(8,128)S(1)}, s32[16,128]{1,0:T(8,128)S(1)}, u32[]{:S(2)}, u32[]{:S(2)}) collective-permute-start(s32[16,128]{1,0:T(8,128)S(1)} %constant_dynamic-update-slice_fusion.refs_0_), channel_id=1, source_target_pairs={{0,6},{2,0},{4,2},{6,4},{8,14},{10,8},{12,10},{14,12},{16,22},{18,... | collective-permute-start | bytes 24584 | tf_op jit(solution)/shard_map/ppermute | solution.py:284
  26.5 4.0 %collective-permute-start.2 = (s32[16,128]{1,0:T(8,128)S(1)}, s32[16,128]{1,0:T(8,128)S(1)}, u32[]{:S(2)}, u32[]{:S(2)}) collective-permute-start(s32[16,128]{1,0:T(8,128)S(1)} %constant_dynamic-update-slice_fusion.refs_0_), channel_id=1, source_target_pairs={{0,4},{2,6},{4,0},{6,2},{8,12},{10,14},{12,8},{14,10},{16,20},{18,... | collective-permute-start | bytes 24584 | tf_op jit(solution)/shard_map/ppermute | solution.py:284
  27.3 4.0 %collective-permute-start.3 = (s32[16,128]{1,0:T(8,128)S(1)}, s32[16,128]{1,0:T(8,128)S(1)}, u32[]{:S(2)}, u32[]{:S(2)}) collective-permute-start(s32[16,128]{1,0:T(8,128)S(1)} %constant_dynamic-update-slice_fusion.refs_0_), channel_id=1, source_target_pairs={{0,2},{2,4},{4,6},{6,0},{8,10},{10,12},{12,14},{14,8},{16,18},{18,... | collective-permute-start | bytes 24584 | tf_op jit(solution)/shard_map/ppermute | solution.py:284
  34.0 4.4 %copy-start.1 = (bf16[384,2048]{1,0:T(8,128)(2,1)S(1)}, bf16[384,2048]{1,0:T(8,128)(2,1)}, u32[]{:S(2)}) copy-start(bf16[384,2048]{1,0:T(8,128)(2,1)} %w_own_ref.1) | copy-start | bytes 4718596
  34.0 7.6 %copy-start.15 = (bf16[2048,24]{0,1:T(8,128)(2,1)S(1)}, bf16[2048,24]{0,1:T(8,128)(2,1)}, u32[]{:S(2)}) copy-start(bf16[2048,24]{0,1:T(8,128)(2,1)} %param.13) | copy-start | bytes 294916
  34.0 16.8 %all-to-all-start = ((bf16[8,576,128]{2,1,0:T(8,128)(2,1)}), bf16[8,576,128]{2,1,0:T(8,128)(2,1)}, u32[]{:S(2)}, u32[]{:S(2)}) async-start(bf16[8,576,128]{2,1,0:T(8,128)(2,1)} %bitcast.2), calls=%async_computation | async-start | bytes 2359296 | tf_op jit(solution)/shard_map/all_to_all | solution.py:303
  38.4 25.6 %collective-permute-start.8 = (bf16[384,2048]{1,0:T(8,128)(2,1)S(1)}, bf16[384,2048]{1,0:T(8,128)(2,1)}, u32[]{:S(2)}, u32[]{:S(2)}) collective-permute-start(bf16[384,2048]{1,0:T(8,128)(2,1)S(1)} %copy-done.1), channel_id=1, source_target_pairs={{0,1},{1,0},{2,3},{3,2},{4,5},{5,4},{6,7},{7,6},{8,9},{9,8},{10,11... | collective-permute-start | bytes 4718600 | tf_op jit(solution)/shard_map/ppermute | solution.py:258
  41.8 1.4 %copy-start.2 = (bf16[2048,384]{1,0:T(8,128)(2,1)S(1)}, bf16[2048,384]{1,0:T(8,128)(2,1)}, u32[]{:S(2)}) copy-start(bf16[2048,384]{1,0:T(8,128)(2,1)} %wq_ref.1) | copy-start | bytes 4718596
  44.8 0.7 %copy-start.9 = (bf16[8,192,128]{2,1,0:T(8,128)(2,1)}, bf16[8,192,128]{2,1,0:T(8,128)(2,1)S(1)}, u32[]{:S(2)}) copy-start(bf16[8,192,128]{2,1,0:T(8,128)(2,1)S(1)} %get-tuple-element.15.plain_ref) | copy-start | bytes 1179652
  45.6 0.8 %copy-start.10 = (bf16[8,192,128]{2,1,0:T(8,128)(2,1)}, bf16[8,192,128]{2,1,0:T(8,128)(2,1)S(1)}, u32[]{:S(2)}) copy-start(bf16[8,192,128]{2,1,0:T(8,128)(2,1)S(1)} %get-tuple-element.16.turned_ref) | copy-start | bytes 1179652
  46.3 0.6 copy-start.11
  50.8 14.4 %copy-start.8 = (f32[2048]{0:T(1024)S(1)}, f32[2048]{0:T(1024)}, u32[]{:S(2)}) copy-start(f32[2048]{0:T(1024)} %param.16) | copy-start | bytes 24580
  59.2 5.9 %collective-permute-start.7 = (bf16[128,384]{1,0:T(8,128)(2,1)}, bf16[128,384]{1,0:T(8,128)(2,1)S(1)}, u32[]{:S(2)}, u32[]{:S(2)}) collective-permute-start(bf16[128,384]{1,0:T(8,128)(2,1)} %get-tuple-element.20), channel_id=1, source_target_pairs={{0,1},{1,0},{2,3},{3,2},{4,5},{5,4},{6,7},{7,6},{8,9},{9,8},{10,11... | collective-permute-start | bytes 294920 | tf_op jit(solution)/shard_map/ppermute | solution.py:322
  65.1 0.9 %copy-start.6 = (bf16[128,384]{1,0:T(8,128)(2,1)S(1)}, bf16[128,384]{1,0:T(8,128)(2,1)}, u32[]{:S(2)}) copy-start(bf16[128,384]{1,0:T(8,128)(2,1)} %get-tuple-element.19.keep_ref) | copy-start | bytes 294916
where the time goes:
time: 69.6 us; the launch traced here: 69.3 us
  starting transfers between devices  27.8 us (40%)
  Pallas kernels  17.4 us (25%)
  waiting for transfers between devices  17.2 us (25%)
  local copies, waits for them, and re-layouts  5.88 us (8%)
  other arithmetic  0.82 us (1%)
    pallas_call x6, Pallas kernels, call(): pl.pallas_call(kernel, out_shape=out_shape, in_specs=specs, out_specs=jax...  17.4 us
    ppermute x3, starting transfers between devices, on_device(): units = [unit] + [lax.ppermute(unit, 'kv', z_shift(d)) for d in (2, 4, 6)]  11.4 us
    ppermute x1, waiting for transfers between devices, on_device(): partner_ask = lax.ppermute(ask, 'kv', z_pair())  8.12 us
    unnamed x34, local copies, waits for them, and re-layouts  5.88 us
    ppermute x1, starting transfers between devices, on_device(): got = lax.ppermute(send, 'tp', [(0, 1), (1, 0)])  4.75 us
    all_to_all x1, starting transfers between devices, on_device(): lax.all_to_all(share.reshape(8, SHARE, 128), 'kv', 0, 0, tiled=True, axis...  4.41 us
    ppermute x3, waiting for transfers between devices, on_device(): asks = [asks] + [lax.ppermute(asks, 'kv', y_shift(-d)) for d in (1, 2, 3)]  4.13 us
    all_to_all x1, waiting for transfers between devices, on_device(): lax.all_to_all(share.reshape(8, SHARE, 128), 'kv', 0, 0, tiled=True, axis...  3.81 us
  transfers between devices with their start and end apart: 10, of which 6 were waited for; matrix products, arithmetic and copies ran while one was open for 0% of the time, Pallas kernels for 15%

commit v1 on v0

--- a/solution.py
+++ b/solution.py
@@ -51,24 +51,30 @@
     out_ref[pl.ds(512, 16), :] = packed.astype(BF)
 
 
-def table_kernel(scalar_ref, listed_ref, ask_ref, rows_ref, bias_ref):
-    z = lax.axis_index("kv") // Y
+def ask_kernel(listed_ref, ask_ref):
     listed = listed_ref[...]
     lane = lax.broadcasted_iota(jnp.int32, (8, 128), 1)
     low, high = jnp.full((8, 128), 7, jnp.int32), jnp.zeros((8, 128), jnp.int32)
+    for t in range(TOPN):
+        entry = jnp.broadcast_to(listed[:, t : t + 1], (8, 128))
+        hit = (entry >> 3) == lane
+        low = jnp.minimum(low, jnp.where(hit, entry & 7, 7))
+        high = jnp.maximum(high, jnp.where(hit, entry & 7, 0))
+    low = jnp.min(low, axis=0, keepdims=True)
+    high = jnp.max(high, axis=0, keepdims=True)
+    first = lax.broadcasted_iota(jnp.int32, (8, 128), 0) == 0
+    ask_ref[...] = jnp.where(first, low, high)
+
+
+def fill_tables(scalar_ref, listed, rows_ref, bias_ref):
+    z = lax.axis_index("kv") // Y
+    lane = lax.broadcasted_iota(jnp.int32, (8, 128), 1)
     for g in range(4):
         row = jnp.zeros((8, 128), F32)
         for part in range(4):
             entry = jnp.broadcast_to(listed[:, g * 4 + part : g * 4 + part + 1], (8, 128))
-            hit = (entry >> 3) == lane
-            low = jnp.minimum(low, jnp.where(hit, entry & 7, 7))
-            high = jnp.maximum(high, jnp.where(hit, entry & 7, 0))
             row = jnp.where((lane >> 5) == part, jnp.where(entry >= 0, 0.0, NEG), row)
         bias_ref[:, pl.ds(g * 128, 128)] = row
-    low = jnp.min(low, axis=0, keepdims=True)
-    high = jnp.max(high, axis=0, keepdims=True)
-    first = lax.broadcasted_iota(jnp.int32, (8, 128), 0) == 0
-    ask_ref[...] = jnp.where(first, low, high)
     owner = listed >> 3
     second = jnp.zeros((8, TOPN), jnp.int32)
     for i in range(8):
@@ -82,27 +88,30 @@
     rows_ref[...] = ((owner_z & 1) * Y + (owner & 3)) * SHARE + u * PIECE + second * BLK
 
 
-def q_kernel(
-    x_ref, wq_ref, wg_hbm, cos_ref, sin_ref, plain_ref, turned_ref, gate_ref, wg_ref, sem
-):
-    copy = pltpu.make_async_copy(wg_hbm, wg_ref, sem)
-    copy.start()
+def q_kernel(scalar_ref, listed_ref, x_ref, wq_ref, wg_ref, cos_ref, sin_ref, *outs):
+    plain_ref, turned_ref, gate_ref, rows_ref, bias_ref = outs
+    fill_tables(scalar_ref, listed_ref[...], rows_ref, bias_ref)
     x = x_ref[...]
+    logits = dot_t(wg_ref[...], x)
+    first_core = lax.axis_index("tp") == 0
+    for branch in range(2):
+        at = branch * 12
+        own = jnp.where(first_core, logits[at : at + 6], logits[at + 6 : at + 12])
+        gate_ref[branch * 8 : branch * 8 + 6, :] = jax.nn.sigmoid(own)
     lane = lax.broadcasted_iota(jnp.int32, (256, 128), 1)
+    plain, turned = [], []
     for pair in range(3):
         q = dot(x, wq_ref[:, pl.ds(pair * 128, 128)]).astype(BF).astype(F32)
-        t = turn(q, cos_ref[...], sin_ref[...]).astype(BF).astype(F32)
-        for half in range(2):
-            head = pair * 2 + half
-            side = head // 3
-            keep = (lane >= HEAD) if side else (lane < HEAD)
-            for src, dst in ((q, plain_ref), (t, turned_ref)):
-                rows = src if half == side else pltpu.roll(src, 64, 1)
-                rows = jnp.where(keep, rows * 0.125, 0.0).astype(BF)
-                for i in range(8):
-                    dst[i, pl.ds(head * BLK, BLK), :] = rows[i * BLK : (i + 1) * BLK]
-    copy.wait()
-    gate_ref[...] = jax.nn.sigmoid(dot(x, wg_ref[...]))
+        plain.append(q * 0.125)
+        turned.append(turn(q, cos_ref[...], sin_ref[...]).astype(BF).astype(F32) * 0.125)
+    for tiles, out in ((plain, plain_ref), (turned, turned_ref)):
+        groups = (
+            jnp.where(lane < HEAD, tiles[0], tiles[1]),
+            jnp.where(lane < HEAD, pltpu.roll(tiles[0], 64, 1), pltpu.roll(tiles[2], 64, 1)),
+            jnp.where(lane < HEAD, tiles[1], tiles[2]),
+        )
+        for g in range(3):
+            out[:, pl.ds(g * 128, 128)] = groups[g].astype(BF)
 
 
 def select_kernel(*refs):
@@ -125,74 +134,101 @@
 def attend_kernel(
     row_ref, bias_ref, plain_ref, turned_ref, gate_ref, unit_ref, pool, *refs
 ):
-    keep_ref, send_ref, sk, sv, kg, vg = refs
+    keep_ref, send_ref, sk, sv, kg, vg, limit_ref, flip_ref = refs
     index = lax.axis_index("kv")
-    z, y, core = index // Y, index % Y, lax.axis_index("tp")
+    z, core = index // Y, lax.axis_index("tp")
+    blocks = [lax.rem(step + 4 * (1 - core), 8) for step in range(8)]
+    starts = [pl.multiple_of(i * BLK, BLK) for i in blocks]
     for piece in range(32):
         base = piece * PIECE + 128
         sk[pl.ds(piece * 8, 8), :] = pool[pl.ds(base, 8), :]
         sv[pl.ds(piece * 8, 8), :] = pool[pl.ds(base + 8, 8), :]
+    for step in range(8):
+        kg[step, pl.ds(0, BLK), :] = unit_ref[pl.ds(starts[step], BLK), :]
+        vg[step, pl.ds(0, BLK), :] = unit_ref[pl.ds(starts[step] + 256, BLK), :]
+        for t in range(1, TOPN):
+            at = pl.multiple_of(row_ref[blocks[step], t], 16)
+            kg[step, pl.ds(t * BLK, BLK), :] = pool[pl.ds(at, BLK), :]
+            vg[step, pl.ds(t * BLK, BLK), :] = pool[pl.ds(at + 64, BLK), :]
 
     column = lax.broadcasted_iota(jnp.int32, (192, 256), 1)
     row = lax.broadcasted_iota(jnp.int32, (192, 256), 0) % BLK
     sender = (z // 2) * 2 + column // 128
     dev = ((sender - 2 * (column // 8 % 4) + Z) % Z) * Y + column // 32 % Y
-    block_id = dev * 8 + column % 8
-    own_first = (z * Y + y) * 8
+    limit_ref[...] = (dev * 8 + column % 8) * BLK + (BLK - 1) - row
     triangle = jnp.where(
         (column[:, :128] < BLK) & (column[:, :128] > row[:, :128]), NEG, 0.0
     )
     lane = lax.broadcasted_iota(jnp.int32, (BLK, 128), 1)
-    coarse_keys, coarse_values = sk[...], sv[...]
-
-    for step in range(8):
-        i = lax.rem(step + 4 * (1 - core), 8)
-        own_row = pl.multiple_of(i * BLK, BLK)
-        kg[step % 2, pl.ds(0, BLK), :] = unit_ref[pl.ds(own_row, BLK), :]
-        vg[step % 2, pl.ds(0, BLK), :] = unit_ref[pl.ds(own_row + 256, BLK), :]
-        for t in range(1, TOPN):
-            at = pl.multiple_of(row_ref[i, t], 16)
-            kg[step % 2, pl.ds(t * BLK, BLK), :] = pool[pl.ds(at, BLK), :]
-            vg[step % 2, pl.ds(t * BLK, BLK), :] = pool[pl.ds(at + 64, BLK), :]
-        scores = dot_t(plain_ref[i], coarse_keys)
-        own = own_first + i
-        visible = (block_id < own) | ((block_id == own) & (row == BLK - 1))
-        scores = jnp.where(visible, scores, NEG)
-        peak = jnp.max(scores, axis=-1, keepdims=True)
-        powers = jnp.where(visible, jnp.exp(scores - peak), 0.0)
+    low = lane < HEAD
+    flip_ref[...] = jnp.transpose(gate_ref[...])
+
+    def heads_of(ref, step):
+        tiles = [ref[pl.ds(starts[step], BLK), pl.ds(g * 128, 128)] for g in range(3)]
+        zero = jnp.zeros_like(tiles[0])
+        return jnp.concatenate(
+            [jnp.where(low, t, zero) for t in tiles] + [jnp.where(low, zero, t) for t in tiles],
+            axis=0,
+        )
+
+    def score(step):
+        return (
+            dot_t(heads_of(plain_ref, step), sk[...]),
+            dot_t(heads_of(turned_ref, step), kg[step]),
+        )
+
+    def finish(step, coarse, fine):
+        own = (index * 8 + blocks[step]) * BLK
+        coarse = jnp.where(limit_ref[...] <= own, coarse, NEG)
+        peak = jnp.maximum(jnp.max(coarse, axis=-1, keepdims=True), NEG * 0.01)
+        powers = jnp.exp(coarse - peak)
         total = jnp.maximum(jnp.sum(powers, axis=-1, keepdims=True), 1.0)
-        weight = (powers * (1.0 / total)).astype(BF)
-        coarse = dot(weight, coarse_values)
-
-        fine = dot_t(turned_ref[i], kg[step % 2]) + bias_ref[pl.ds(i, 1), :]
+        coarse_out = dot((powers * (1.0 / total)).astype(BF), sv[...])
+
+        fine = fine + bias_ref[pl.ds(blocks[step], 1), :]
         fine = jnp.concatenate([fine[:, :128] + triangle, fine[:, 128:]], axis=1)
-        fine_peak = jnp.max(fine, axis=-1, keepdims=True)
-        fine_powers = jnp.exp(fine - fine_peak)
-        fine_total = jnp.sum(fine_powers, axis=-1, keepdims=True)
-        fine_out = dot(fine_powers.astype(BF), vg[step % 2]) * (1.0 / fine_total)
-
-        gates = gate_ref[pl.ds(pl.multiple_of(i * BLK, BLK), BLK), :]
-        heads = []
-        for head in range(6):
-            pick = []
-            for base in (0, 12):
-                low = gates[:, base + head : base + head + 1]
-                high = gates[:, base + 6 + head : base + 7 + head]
-                pick.append(jnp.where(core == 0, low, high))
-            span = slice(head * BLK, (head + 1) * BLK)
-            heads.append(pick[0] * coarse[span] + pick[1] * fine_out[span])
-        groups = (
-            jnp.where(lane < HEAD, heads[0], pltpu.roll(heads[1], 64, 1)),
-            jnp.where(lane < HEAD, heads[2], heads[3]),
-            jnp.where(lane < HEAD, pltpu.roll(heads[4], 64, 1), heads[5]),
-        )
+        fine_powers = jnp.exp(fine - jnp.max(fine, axis=-1, keepdims=True))
+        inverse = 1.0 / jnp.sum(fine_powers, axis=-1, keepdims=True)
+        fine_out = dot(fine_powers.astype(BF), vg[step])
+
+        gates = flip_ref[pl.ds(starts[step], BLK), :]
         target = send_ref if step < 4 else keep_ref
         for g in range(3):
-            target[pl.ds((step % 4) * BLK, BLK), pl.ds(g * 128, 128)] = groups[g].astype(BF)
-
-
-def out_kernel(keep_ref, got_ref, w_own_ref, w_other_ref, gain_ref, out_ref):
-    summed = dot(keep_ref[...], w_own_ref[...]) + dot(got_ref[...], w_other_ref[...])
+            a, b = g * BLK, (3 + g) * BLK
+            gate = jnp.where(low, gates[:, g : g + 1], gates[:, 3 + g : 4 + g])
+            fine_gate = jnp.where(
+                low,
+                gates[:, 8 + g : 9 + g] * inverse[a : a + BLK],
+                gates[:, 11 + g : 12 + g] * inverse[b : b + BLK],
+            )
+            mixed = gate * jnp.where(low, coarse_out[a : a + BLK], coarse_out[b : b + BLK])
+            mixed += fine_gate * jnp.where(low, fine_out[a : a + BLK], fine_out[b : b + BLK])
+            target[pl.ds((step % 4) * BLK, BLK), pl.ds(g * 128, 128)] = mixed.astype(BF)
+
+    ahead = score(0)
+    for step in range(8):
+        now, ahead = ahead, score(step + 1) if step < 7 else None
+        finish(step, *now)
+
+
+def by_group(mixed_ref, weight_ref):
+    total = None
+    for g in range(3):
+        weight = jnp.concatenate(
+            [weight_ref[pl.ds(g * HEAD, HEAD), :], weight_ref[pl.ds((3 + g) * HEAD, HEAD), :]],
+            axis=0,
+        )
+        part = dot(mixed_ref[:, pl.ds(g * 128, 128)], weight)
+        total = part if total is None else total + part
+    return total
+
+
+def kept_kernel(keep_ref, weight_ref, out_ref):
+    out_ref[...] = by_group(keep_ref, weight_ref)
+
+
+def out_kernel(part_ref, got_ref, weight_ref, gain_ref, out_ref):
+    summed = part_ref[...] + by_group(got_ref, weight_ref)
     mean = jnp.mean(summed * summed, axis=-1, keepdims=True)
     out_ref[...] = summed * lax.rsqrt(mean + EPS) * gain_ref[...]
 
@@ -256,17 +292,8 @@
     x = tokens[0]
     index = lax.axis_index("kv")
     other_weight = lax.ppermute(out_weight, "tp", [(0, 1), (1, 0)])
-    ask, rows, bias = call(
-        table_kernel,
-        (
-            shape((8, 128), jnp.int32),
-            shape((8, TOPN), jnp.int32),
-            shape((8, TOPN * BLK), F32),
-        ),
-        [SMEM, VMEM],
-        (chosen[0], chosen[0]),
-        flops=2**32,
-        data=2**12,
+    ask = call(
+        ask_kernel, shape((8, 128), jnp.int32), [VMEM], (chosen[0],), flops=2**32, data=2**12
     )
     partner_ask = lax.ppermute(ask, "kv", z_pair())
 
@@ -283,12 +310,17 @@
     asks = jnp.concatenate([ask, partner_ask])
     asks = [asks] + [lax.ppermute(asks, "kv", y_shift(-d)) for d in (1, 2, 3)]
 
-    plain, turned, gates = call(
+    plain, turned, gates, rows, bias = call(
         q_kernel,
-        (shape((8, 192, 128), BF), shape((8, 192, 128), BF), shape((256, 24), F32)),
-        [VMEM, VMEM, HBM, VMEM, VMEM],
-        (x, query_weight, gate_weight, cosine, sine),
-        scratch=[pltpu.VMEM(gate_weight.shape, BF), pltpu.SemaphoreType.DMA],
+        (
+            shape((256, 384), BF),
+            shape((256, 384), BF),
+            shape((16, 256), F32),
+            shape((8, TOPN), jnp.int32),
+            shape((8, TOPN * BLK), F32),
+        ),
+        [SMEM] + [VMEM] * 6,
+        (chosen[0], chosen[0], x, query_weight, gate_weight.T, cosine, sine),
         flops=2 * 256 * 2048 * 408,
         data=3 * 2**20,
     )
@@ -312,20 +344,30 @@
         scratch=[
             pltpu.VMEM((256, 128), BF),
             pltpu.VMEM((256, 128), BF),
-            pltpu.VMEM((2, 512, 128), BF),
-            pltpu.VMEM((2, 512, 128), BF),
+            pltpu.VMEM((8, 512, 128), BF),
+            pltpu.VMEM((8, 512, 128), BF),
+            pltpu.VMEM((192, 256), jnp.int32),
+            pltpu.VMEM((256, 16), F32),
         ],
         flops=2**30,
         data=4 * 2**20,
-        vmem=58720256,
+        vmem=12 * 2**20,
     )
     got = lax.ppermute(send, "tp", [(0, 1), (1, 0)])
+    part = call(
+        kept_kernel,
+        shape((128, 2048), F32),
+        [VMEM] * 2,
+        (keep, out_weight),
+        flops=2 * 128 * 384 * 2048,
+        data=3 * 2**20,
+    )
     out = call(
         out_kernel,
         shape((128, 2048), F32),
-        [VMEM] * 5,
-        (keep, got, out_weight, other_weight, out_gain[None]),
-        flops=2 * 128 * 768 * 2048,
+        [VMEM] * 4,
+        (part, got, other_weight, out_gain[None]),
+        flops=2 * 128 * 384 * 2048,
         data=4 * 2**20,
     )
     return out[None]

time: 69.6 us -> 63 us (0.905)
  Pallas kernels: 17.4 us -> 13.3 us
  local copies, waits for them, and re-layouts: 5.88 us -> 2.76 us
  starting transfers between devices: 27.8 us -> 30.5 us
  waiting for transfers between devices: 17.2 us -> 15.3 us
    pallas_call x6 -> x7, Pallas kernels: 17.4 us -> 13.3 us  [call(): pl.pallas_call(kernel, out_shape=out_shape, in_specs=specs, out_specs=jax...]
    unnamed x34 -> x20, local copies, waits for them, and re-layouts: 5.88 us -> 2.76 us
    ppermute x3, waiting for transfers between devices: 4.13 us -> 1.48 us  [on_device(): asks = [asks] + [lax.ppermute(asks, 'kv', y_shift(-d)) for d in (1, 2, 3)]]
    ppermute x3, starting transfers between devices: 3.35 us -> 5.23 us  [on_device(): asks = [asks] + [lax.ppermute(asks, 'kv', y_shift(-d)) for d in (1, 2, 3)]]
    all_to_all x1, waiting for transfers between devices: 3.81 us -> 5.62 us  [on_device(): lax.all_to_all(share.reshape(8, SHARE, 128), 'kv', 0, 0, tiled=True, axis...]
    all_to_all x1, starting transfers between devices: 4.41 us -> 6.03 us  [on_device(): lax.all_to_all(share.reshape(8, SHARE, 128), 'kv', 0, 0, tiled=True, axis...]
    ppermute x3, starting transfers between devices: 11.4 us -> 10.2 us  [on_device(): units = [unit] + [lax.ppermute(unit, 'kv', z_shift(d)) for d in (2, 4, 6)]]
    ppermute x1, waiting for transfers between devices: 1.15 us -> 0.38 us  [on_device(): got = lax.ppermute(send, 'tp', [(0, 1), (1, 0)])]
  transfers between devices with their start and end apart: 10 -> 10, of which waited for: 6 -> 5; matrix products, arithmetic and copies ran while one was open for 0% -> 0% of each run, Pallas kernels for 15% -> 13%
where the time goes in v1:
time: 63 us; the launch traced here: 62.7 us
  starting transfers between devices  30.5 us (48%)
  waiting for transfers between devices  15.3 us (24%)
  Pallas kernels  13.3 us (21%)
  local copies, waits for them, and re-layouts  2.76 us (4%)
  other arithmetic  0.82 us (1%)
    pallas_call x7, Pallas kernels, call(): pl.pallas_call(kernel, out_shape=out_shape, in_specs=specs, out_specs=jax...  13.3 us
    ppermute x3, starting transfers between devices, on_device(): units = [unit] + [lax.ppermute(unit, 'kv', z_shift(d)) for d in (2, 4, 6)]  10.2 us
    ppermute x1, waiting for transfers between devices, on_device(): partner_ask = lax.ppermute(ask, 'kv', z_pair())  7.79 us
    all_to_all x1, starting transfers between devices, on_device(): lax.all_to_all(share.reshape(8, SHARE, 128), 'kv', 0, 0, tiled=True, axis...  6.03 us
    all_to_all x1, waiting for transfers between devices, on_device(): lax.all_to_all(share.reshape(8, SHARE, 128), 'kv', 0, 0, tiled=True, axis...  5.62 us
    ppermute x3, starting transfers between devices, on_device(): asks = [asks] + [lax.ppermute(asks, 'kv', y_shift(-d)) for d in (1, 2, 3)]  5.23 us
    ppermute x1, starting transfers between devices, on_device(): got = lax.ppermute(send, 'tp', [(0, 1), (1, 0)])  5.15 us
    ppermute x1, starting transfers between devices, on_device(): other_weight = lax.ppermute(out_weight, 'tp', [(0, 1), (1, 0)])  3.17 us
  transfers between devices with their start and end apart: 10, of which 5 were waited for; matrix products, arithmetic and copies ran while one was open for 0% of the time, Pallas kernels for 13%

profile of v1, /device:TPU:1, one launch (start us, length us, event | category | flops | bytes accessed | tf_op | source)
XLA Modules:
  0.0 62.7 jit_solution(8739728701335576334)
XLA Ops:
  0.0 0.0 copy-start.7
  0.0 0.7 %copy-done.7 = s32[1,8,16]{2,1,0:T(8,128)S(1)} copy-done((s32[1,8,16]{2,1,0:T(8,128)S(1)}, s32[1,8,16]{2,1,0:T(8,128)}, u32[]{:S(2)}) %copy-start.7) | copy-done | bytes 536
  0.7 0.0 copy-start.3
  0.7 0.0 copy-start.4
  0.7 0.0 copy-start.6
  0.7 0.1 shard_map.92.after_ref
  0.8 0.0 copy-start
  0.8 0.5 fusion
  1.4 0.3 pad_maximum_fusion
  1.7 0.1 copy-done.3
  1.8 0.2 copy-done.4
  1.9 0.0 copy-done.6
  1.9 0.4 copy-done
  2.3 0.7 %shard_map.93.refs_4_.unit_ref = bf16[528,128]{1,0:T(8,128)(2,1)S(1)} custom-call(s32[8,128]{1,0:T(8,128)S(1)} %shard_map.92.after_ref, bf16[256,2048]{1,0:T(8,128)(2,1)S(1)} %bitcast.7, bf16[2048,128]{1,0:T(8,128)(2,1)S(1)} %copy-done.3, bf16[2048,128]{1,0:T(8,128)(2,1)S(1)} %copy-done.4, f32[2,32,64]{2,1,0:T(8,128)S(1)} %copy-done.6, ...), custom_call_target="tpu_custom_call" | custom-call | flops 268435456 | bytes 2097152 | tf_op jit(solution)/shard_map/pallas_call | solution.py:242
  3.0 6.9 %collective-permute-start.6 = (bf16[528,128]{1,0:T(8,128)(2,1)S(1)}, bf16[528,128]{1,0:T(8,128)(2,1)S(1)}, u32[]{:S(2)}, u32[]{:S(2)}) collective-permute-start(bf16[528,128]{1,0:T(8,128)(2,1)S(1)} %shard_map.93.refs_4_.unit_ref), channel_id=1, source_target_pairs={{0,48},{2,50},{4,52},{6,54},{8,56},{10,58},{12,60},{14,62},{16,0},... | collective-permute-start | bytes 405512 | tf_op jit(solution)/shard_map/ppermute | solution.py:309
  9.9 1.0 %collective-permute-start.5 = (bf16[528,128]{1,0:T(8,128)(2,1)S(1)}, bf16[528,128]{1,0:T(8,128)(2,1)S(1)}, u32[]{:S(2)}, u32[]{:S(2)}) collective-permute-start(bf16[528,128]{1,0:T(8,128)(2,1)S(1)} %shard_map.93.refs_4_.unit_ref), channel_id=1, source_target_pairs={{0,32},{2,34},{4,36},{6,38},{8,40},{10,42},{12,44},{14,46},{16,48}... | collective-permute-start | bytes 405512 | tf_op jit(solution)/shard_map/ppermute | solution.py:309
  10.9 2.3 %collective-permute-start.4 = (bf16[528,128]{1,0:T(8,128)(2,1)S(1)}, bf16[528,128]{1,0:T(8,128)(2,1)S(1)}, u32[]{:S(2)}, u32[]{:S(2)}) collective-permute-start(bf16[528,128]{1,0:T(8,128)(2,1)S(1)} %shard_map.93.refs_4_.unit_ref), channel_id=1, source_target_pairs={{0,16},{2,18},{4,20},{6,22},{8,24},{10,26},{12,28},{14,30},{16,32}... | collective-permute-start | bytes 405512 | tf_op jit(solution)/shard_map/ppermute | solution.py:309
  13.2 0.7 %collective-permute-start = (s32[8,128]{1,0:T(8,128)S(1)}, s32[8,128]{1,0:T(8,128)S(1)}, u32[]{:S(2)}, u32[]{:S(2)}) collective-permute-start(s32[8,128]{1,0:T(8,128)S(1)} %shard_map.92.after_ref), channel_id=1, source_target_pairs={{0,8},{2,10},{4,12},{6,14},{8,0},{10,2},{12,4},{14,6},{16,24},{18,... | collective-permute-start | bytes 12296 | tf_op jit(solution)/shard_map/ppermute | solution.py:298
  13.9 7.8 %collective-permute-done = s32[8,128]{1,0:T(8,128)S(1)} collective-permute-done((s32[8,128]{1,0:T(8,128)S(1)}, s32[8,128]{1,0:T(8,128)S(1)}, u32[]{:S(2)}, u32[]{:S(2)}) %collective-permute-start) | collective-permute-done | bytes 4128 | tf_op jit(solution)/shard_map/ppermute | solution.py:298
  21.7 1.3 %collective-permute-start.3 = (s32[16,128]{1,0:T(8,128)S(1)}, s32[16,128]{1,0:T(8,128)S(1)}, u32[]{:S(2)}, u32[]{:S(2)}) collective-permute-start(s32[16,128]{1,0:T(8,128)S(1)} %pad_add_fusion.refs_0_), channel_id=1, source_target_pairs={{0,2},{2,4},{4,6},{6,0},{8,10},{10,12},{12,14},{14,8},{16,18},{18,... | collective-permute-start | bytes 24584 | tf_op jit(solution)/shard_map/ppermute | solution.py:311
  23.0 2.6 %collective-permute-start.2 = (s32[16,128]{1,0:T(8,128)S(1)}, s32[16,128]{1,0:T(8,128)S(1)}, u32[]{:S(2)}, u32[]{:S(2)}) collective-permute-start(s32[16,128]{1,0:T(8,128)S(1)} %pad_add_fusion.refs_0_), channel_id=1, source_target_pairs={{0,4},{2,6},{4,0},{6,2},{8,12},{10,14},{12,8},{14,10},{16,20},{18,... | collective-permute-start | bytes 24584 | tf_op jit(solution)/shard_map/ppermute | solution.py:311
  25.6 0.0 collective-permute-done.3.refs_3_
  25.6 1.3 %collective-permute-start.1 = (s32[16,128]{1,0:T(8,128)S(1)}, s32[16,128]{1,0:T(8,128)S(1)}, u32[]{:S(2)}, u32[]{:S(2)}) collective-permute-start(s32[16,128]{1,0:T(8,128)S(1)} %pad_add_fusion.refs_0_), channel_id=1, source_target_pairs={{0,6},{2,0},{4,2},{6,4},{8,14},{10,8},{12,10},{14,12},{16,22},{18,... | collective-permute-start | bytes 24584 | tf_op jit(solution)/shard_map/ppermute | solution.py:311
  27.0 0.1 collective-permute-done.2.refs_2_
  27.0 1.4 %collective-permute-done.1.refs_1_ = s32[16,128]{1,0:T(8,128)S(1)} collective-permute-done((s32[16,128]{1,0:T(8,128)S(1)}, s32[16,128]{1,0:T(8,128)S(1)}, u32[]{:S(2)}, u32[]{:S(2)}) %collective-permute-start.1) | collective-permute-done | bytes 8224 | tf_op jit(solution)/shard_map/ppermute | solution.py:311
  28.4 0.0 collective-permute-done.6.refs_7_
  28.4 0.0 collective-permute-done.5.refs_6_
  28.4 0.0 collective-permute-done.4.refs_5_
  28.4 2.6 %shard_map.94 = bf16[4608,128]{1,0:T(8,128)(2,1)} custom-call(s32[16,128]{1,0:T(8,128)S(1)} %pad_add_fusion.refs_0_, s32[16,128]{1,0:T(8,128)S(1)} %collective-permute-done.1.refs_1_, s32[16,128]{1,0:T(8,128)S(1)} %collective-permute-done.2.refs_2_, s32[16,128]{1,0:T(8,128)S(1)} %collective-permute-done.3.refs_3_, ...), custom_call_target="tpu_custom_call" | custom-call | flops 1048576 | bytes 2097152 | tf_op jit(solution)/shard_map/pallas_call | solution.py:242
  31.1 0.0 copy-start.5
  31.1 0.0 copy-start.8
  31.1 6.0 %all-to-all-start = ((bf16[8,576,128]{2,1,0:T(8,128)(2,1)}), bf16[8,576,128]{2,1,0:T(8,128)(2,1)}, u32[]{:S(2)}, u32[]{:S(2)}) async-start(bf16[8,576,128]{2,1,0:T(8,128)(2,1)} %bitcast.3), calls=%async_computation | async-start | bytes 2359296 | tf_op jit(solution)/shard_map/all_to_all | solution.py:335
  37.1 3.2 %collective-permute-start.8 = (bf16[384,2048]{1,0:T(8,128)(2,1)}, bf16[384,2048]{1,0:T(8,128)(2,1)S(1)}, u32[]{:S(2)}, u32[]{:S(2)}) collective-permute-start(bf16[384,2048]{1,0:T(8,128)(2,1)} %weight_ref.1), channel_id=1, source_target_pairs={{0,1},{1,0},{2,3},{3,2},{4,5},{5,4},{6,7},{7,6},{8,9},{9,8},{10,11... | collective-permute-start | bytes 4718600 | tf_op jit(solution)/shard_map/ppermute | solution.py:294
  40.3 0.0 copy-done.5
  40.3 0.0 copy-done.8
  40.3 0.0 copy-start.1
  40.3 1.4 %copy-done.1 = bf16[2048,384]{1,0:T(8,128)(2,1)S(1)} copy-done((bf16[2048,384]{1,0:T(8,128)(2,1)S(1)}, bf16[2048,384]{1,0:T(8,128)(2,1)}, u32[]{:S(2)}) %copy-start.1) | copy-done | bytes 1572888
  41.7 2.0 %shard_map.91 = (bf16[256,384]{1,0:T(8,128)(2,1)S(1)}, bf16[256,384]{1,0:T(8,128)(2,1)S(1)}, f32[16,256]{1,0:T(8,128)S(1)}, s32[8,16]{1,0:T(8,128)S(1)}, f32[8,512]{1,0:T(8,128)S(1)}) custom-call(s32[8,16]{1,0:T(8,128)S(1)} %bitcast.11, s32[8,16]{1,0:T(8,128)S(1)} %bitcast.12, bf16[256,2048]{1,0:T(8,128)(2,1)S(1)} %bitcast.8, ...), custom_call_target="tpu_custom_call" | custom-call | flops 427819008 | bytes 3145728 | tf_op jit(solution)/shard_map/pallas_call | solution.py:242
  43.7 5.6 %all-to-all-done = bf16[8,576,128]{2,1,0:T(8,128)(2,1)} async-done(((bf16[8,576,128]{2,1,0:T(8,128)(2,1)}), bf16[8,576,128]{2,1,0:T(8,128)(2,1)}, u32[]{:S(2)}, u32[]{:S(2)}) %all-to-all-start) | async-done | bytes 1179680 | tf_op jit(solution)/shard_map/all_to_all | solution.py:335
  49.3 5.6 %shard_map.95 = (bf16[128,384]{1,0:T(8,128)(2,1)S(1)}, bf16[128,384]{1,0:T(8,128)(2,1)S(1)}) custom-call(s32[8,16]{1,0:T(8,128)S(1)} %get-tuple-element.12.row_ref, f32[8,512]{1,0:T(8,128)S(1)} %get-tuple-element.13.bias_ref, bf16[256,384]{1,0:T(8,128)(2,1)S(1)} %get-tuple-element.14.plain_ref, bf16[256,384]{1,0:T(8,128)(2,1)S(1)} %get-tuple-element.15.turned_ref, ...), custom_call_target="tpu_custom_call" | custom-call | flops 1073741824 | bytes 4194304 | tf_op jit(solution)/shard_map/pallas_call | solution.py:242
  54.9 0.0 copy-start.9
  54.9 5.1 %collective-permute-start.7 = (bf16[128,384]{1,0:T(8,128)(2,1)S(1)}, bf16[128,384]{1,0:T(8,128)(2,1)S(1)}, u32[]{:S(2)}, u32[]{:S(2)}) collective-permute-start(bf16[128,384]{1,0:T(8,128)(2,1)S(1)} %get-tuple-element.18), channel_id=1, source_target_pairs={{0,1},{1,0},{2,3},{3,2},{4,5},{5,4},{6,7},{7,6},{8,9},{9,8},{10,11... | collective-permute-start | bytes 294920 | tf_op jit(solution)/shard_map/ppermute | solution.py:356
  60.1 0.0 copy-done.2
  60.1 0.6 shard_map.96.part_ref
  60.6 0.0 collective-permute-done.8.weight_ref
  60.6 0.4 collective-permute-done.7.got_ref
  61.0 0.0 copy-done.9
  61.0 1.7 %shard_map.97 = f32[128,2048]{1,0:T(8,128)} custom-call(f32[128,2048]{1,0:T(8,128)S(1)} %shard_map.96.part_ref, bf16[128,384]{1,0:T(8,128)(2,1)S(1)} %collective-permute-done.7.got_ref, bf16[384,2048]{1,0:T(8,128)(2,1)S(1)} %collective-permute-done.8.weight_ref, f32[1,2048]{1,0:T(1,128)S(1)} %bitcast.13), custom_call_target="tpu_custom_call" | custom-call | flops 201326592 | bytes 4194304 | tf_op jit(solution)/shard_map/pallas_call | solution.py:242
  (4 shorter events, 0.0 us)
Async XLA Ops:
  0.0 0.7 %copy-start.7 = (s32[1,8,16]{2,1,0:T(8,128)S(1)}, s32[1,8,16]{2,1,0:T(8,128)}, u32[]{:S(2)}) copy-start(s32[1,8,16]{2,1,0:T(8,128)} %param.17) | copy-start | bytes 1540
  0.7 1.0 %copy-start.3 = (bf16[2048,128]{1,0:T(8,128)(2,1)S(1)}, bf16[2048,128]{1,0:T(8,128)(2,1)}, u32[]{:S(2)}) copy-start(bf16[2048,128]{1,0:T(8,128)(2,1)} %wk_ref.1) | copy-start | bytes 1572868
  0.7 1.2 %copy-start.4 = (bf16[2048,128]{1,0:T(8,128)(2,1)S(1)}, bf16[2048,128]{1,0:T(8,128)(2,1)}, u32[]{:S(2)}) copy-start(bf16[2048,128]{1,0:T(8,128)(2,1)} %wv_ref.1) | copy-start | bytes 1572868
  0.7 1.2 %copy-start.6 = (f32[2,32,64]{2,1,0:T(8,128)S(1)}, f32[2,32,64]{2,1,0:T(8,128)}, u32[]{:S(2)}) copy-start(f32[2,32,64]{2,1,0:T(8,128)} %cw_ref.1) | copy-start | bytes 49156
  0.8 1.5 %copy-start = (bf16[1,256,2048]{2,1,0:T(8,128)(2,1)S(1)}, bf16[1,256,2048]{2,1,0:T(8,128)(2,1)}, u32[]{:S(2)}) copy-start(bf16[1,256,2048]{2,1,0:T(8,128)(2,1)} %param.9) | copy-start | bytes 3145732
  3.0 25.4 %collective-permute-start.6 = (bf16[528,128]{1,0:T(8,128)(2,1)S(1)}, bf16[528,128]{1,0:T(8,128)(2,1)S(1)}, u32[]{:S(2)}, u32[]{:S(2)}) collective-permute-start(bf16[528,128]{1,0:T(8,128)(2,1)S(1)} %shard_map.93.refs_4_.unit_ref), channel_id=1, source_target_pairs={{0,48},{2,50},{4,52},{6,54},{8,56},{10,58},{12,60},{14,62},{16,0},... | collective-permute-start | bytes 405512 | tf_op jit(solution)/shard_map/ppermute | solution.py:309
  9.9 18.5 %collective-permute-start.5 = (bf16[528,128]{1,0:T(8,128)(2,1)S(1)}, bf16[528,128]{1,0:T(8,128)(2,1)S(1)}, u32[]{:S(2)}, u32[]{:S(2)}) collective-permute-start(bf16[528,128]{1,0:T(8,128)(2,1)S(1)} %shard_map.93.refs_4_.unit_ref), channel_id=1, source_target_pairs={{0,32},{2,34},{4,36},{6,38},{8,40},{10,42},{12,44},{14,46},{16,48}... | collective-permute-start | bytes 405512 | tf_op jit(solution)/shard_map/ppermute | solution.py:309
  10.9 17.5 %collective-permute-start.4 = (bf16[528,128]{1,0:T(8,128)(2,1)S(1)}, bf16[528,128]{1,0:T(8,128)(2,1)S(1)}, u32[]{:S(2)}, u32[]{:S(2)}) collective-permute-start(bf16[528,128]{1,0:T(8,128)(2,1)S(1)} %shard_map.93.refs_4_.unit_ref), channel_id=1, source_target_pairs={{0,16},{2,18},{4,20},{6,22},{8,24},{10,26},{12,28},{14,30},{16,32}... | collective-permute-start | bytes 405512 | tf_op jit(solution)/shard_map/ppermute | solution.py:309
  13.2 8.5 %collective-permute-start = (s32[8,128]{1,0:T(8,128)S(1)}, s32[8,128]{1,0:T(8,128)S(1)}, u32[]{:S(2)}, u32[]{:S(2)}) collective-permute-start(s32[8,128]{1,0:T(8,128)S(1)} %shard_map.92.after_ref), channel_id=1, source_target_pairs={{0,8},{2,10},{4,12},{6,14},{8,0},{10,2},{12,4},{14,6},{16,24},{18,... | collective-permute-start | bytes 12296 | tf_op jit(solution)/shard_map/ppermute | solution.py:298
  21.7 3.9 %collective-permute-start.3 = (s32[16,128]{1,0:T(8,128)S(1)}, s32[16,128]{1,0:T(8,128)S(1)}, u32[]{:S(2)}, u32[]{:S(2)}) collective-permute-start(s32[16,128]{1,0:T(8,128)S(1)} %pad_add_fusion.refs_0_), channel_id=1, source_target_pairs={{0,2},{2,4},{4,6},{6,0},{8,10},{10,12},{12,14},{14,8},{16,18},{18,... | collective-permute-start | bytes 24584 | tf_op jit(solution)/shard_map/ppermute | solution.py:311
  23.0 4.0 %collective-permute-start.2 = (s32[16,128]{1,0:T(8,128)S(1)}, s32[16,128]{1,0:T(8,128)S(1)}, u32[]{:S(2)}, u32[]{:S(2)}) collective-permute-start(s32[16,128]{1,0:T(8,128)S(1)} %pad_add_fusion.refs_0_), channel_id=1, source_target_pairs={{0,4},{2,6},{4,0},{6,2},{8,12},{10,14},{12,8},{14,10},{16,20},{18,... | collective-permute-start | bytes 24584 | tf_op jit(solution)/shard_map/ppermute | solution.py:311
  25.6 2.8 %collective-permute-start.1 = (s32[16,128]{1,0:T(8,128)S(1)}, s32[16,128]{1,0:T(8,128)S(1)}, u32[]{:S(2)}, u32[]{:S(2)}) collective-permute-start(s32[16,128]{1,0:T(8,128)S(1)} %pad_add_fusion.refs_0_), channel_id=1, source_target_pairs={{0,6},{2,0},{4,2},{6,4},{8,14},{10,8},{12,10},{14,12},{16,22},{18,... | collective-permute-start | bytes 24584 | tf_op jit(solution)/shard_map/ppermute | solution.py:311
  31.1 9.2 %copy-start.5 = (bf16[2048,24]{0,1:T(8,128)(2,1)S(1)}, bf16[2048,24]{0,1:T(8,128)(2,1)}, u32[]{:S(2)}) copy-start(bf16[2048,24]{0,1:T(8,128)(2,1)} %param.13) | copy-start | bytes 294916
  31.1 9.2 %copy-start.8 = (s32[1,8,16]{2,1,0:T(8,128)S(1)}, s32[1,8,16]{2,1,0:T(8,128)}, u32[]{:S(2)}) copy-start(s32[1,8,16]{2,1,0:T(8,128)} %param.17) | copy-start | bytes 1540
  31.1 18.2 %all-to-all-start = ((bf16[8,576,128]{2,1,0:T(8,128)(2,1)}), bf16[8,576,128]{2,1,0:T(8,128)(2,1)}, u32[]{:S(2)}, u32[]{:S(2)}) async-start(bf16[8,576,128]{2,1,0:T(8,128)(2,1)} %bitcast.3), calls=%async_computation | async-start | bytes 2359296 | tf_op jit(solution)/shard_map/all_to_all | solution.py:335
  37.1 23.5 %collective-permute-start.8 = (bf16[384,2048]{1,0:T(8,128)(2,1)}, bf16[384,2048]{1,0:T(8,128)(2,1)S(1)}, u32[]{:S(2)}, u32[]{:S(2)}) collective-permute-start(bf16[384,2048]{1,0:T(8,128)(2,1)} %weight_ref.1), channel_id=1, source_target_pairs={{0,1},{1,0},{2,3},{3,2},{4,5},{5,4},{6,7},{7,6},{8,9},{9,8},{10,11... | collective-permute-start | bytes 4718600 | tf_op jit(solution)/shard_map/ppermute | solution.py:294
  40.3 1.4 %copy-start.1 = (bf16[2048,384]{1,0:T(8,128)(2,1)S(1)}, bf16[2048,384]{1,0:T(8,128)(2,1)}, u32[]{:S(2)}) copy-start(bf16[2048,384]{1,0:T(8,128)(2,1)} %wq_ref.1) | copy-start | bytes 4718596
  49.3 10.8 %copy-start.2 = (bf16[384,2048]{1,0:T(8,128)(2,1)S(1)}, bf16[384,2048]{1,0:T(8,128)(2,1)}, u32[]{:S(2)}) copy-start(bf16[384,2048]{1,0:T(8,128)(2,1)} %weight_ref.1) | copy-start | bytes 4718596
  54.9 6.1 %copy-start.9 = (f32[2048]{0:T(1024)S(1)}, f32[2048]{0:T(1024)}, u32[]{:S(2)}) copy-start(f32[2048]{0:T(1024)} %param.16) | copy-start | bytes 24580
  54.9 6.1 %collective-permute-start.7 = (bf16[128,384]{1,0:T(8,128)(2,1)S(1)}, bf16[128,384]{1,0:T(8,128)(2,1)S(1)}, u32[]{:S(2)}, u32[]{:S(2)}) collective-permute-start(bf16[128,384]{1,0:T(8,128)(2,1)S(1)} %get-tuple-element.18), channel_id=1, source_target_pairs={{0,1},{1,0},{2,3},{3,2},{4,5},{5,4},{6,7},{7,6},{8,9},{9,8},{10,11... | collective-permute-start | bytes 294920 | tf_op jit(solution)/shard_map/ppermute | solution.py:356
